TPU v7x, 32 devices: a whole 2x2x4 slice. The times are simulated.
32 devices in a mesh: dp: 4 (over y, x), kv: 4 (over z), tp: 2 (over core).
Axes of the slice: x: 2, y: 2, z: 4, core: 2. Of those that a mesh axis runs over, the one named last changes fastest.
Arguments:
- tokens: bfloat16 [4, 16, 2048], P('dp', None, 'kv'), may hold values from -18 to 18, as said below
- norm_gain: float32 [2048], P('kv'), may hold values from 0.1 to 1.9
- w_query: bfloat16 [2048, 3072], P('kv', 'tp'), may hold values from -0.125 to 0.125
- w_key: bfloat16 [2048, 3072], P('kv', 'tp'), may hold values from -0.125 to 0.125
- w_value: bfloat16 [2048, 3072], P('kv', 'tp'), may hold values from -0.125 to 0.125
- w_gate: bfloat16 [2048, 3072], P('kv', 'tp'), may hold values from -0.125 to 0.125
- w_out: bfloat16 [3072, 2048], P('tp', 'kv'), may hold values from -0.109375 to 0.109375
- head_bias: float32 [24], P('tp'), may hold values from -14 to -2
- cache_keys: bfloat16 [4, 2048, 24, 128], P('dp', 'kv', 'tp'), may hold values from -18 to 18, as said below
- cache_values: bfloat16 [4, 2048, 24, 128], P('dp', 'kv', 'tp'), may hold values from -6 to 6
- prefix_len: int32 [4], P('dp'), may hold values from 1536 to 2028
- accepted: int32 [4], P('dp'), may hold values from 1 to 4
- parent: int32 [4, 16], P('dp'), may hold values from -1 to 14, as said below
Outputs:
- mixed: bfloat16 [4, 16, 2048], P('dp', None, 'kv')
- keys_next: bfloat16 [4, 2048, 24, 128], P('dp', 'kv', 'tp')
- values_next: bfloat16 [4, 2048, 24, 128], P('dp', 'kv', 'tp')
Inputs may be any that keep to these rules, and one draw needn't show every extreme that they name: `tokens`: entries of order one. `cache_keys`: entries of order one. parent of proposal 0 is -1; for p of 1 or more, parent[p] lies in max(p - 3, 0) to p - 1.
All inputs are finite; a program needn't handle non-finite values.
Results may differ from a plain program's by a relative error of at most 0.012.
Values may be sent and summed in bfloat16 or wider, within the bound.
A program may use at most 64 MiB of HBM per device.

v0:
```python
import jax
import jax.numpy as jnp
from jax import lax
from jax.sharding import PartitionSpec as P

D = 2048
HEAD = 128


EPS = 1e-06


def ancestry(parent):
    count = parent.shape[-1]
    places = jnp.arange(count, dtype=jnp.int32)
    reach = (parent[:, :, None] == places[None, None, :]).astype(jnp.float32)
    for repeat in range(count.bit_length()):
        reach = jnp.minimum(
            reach + jnp.einsum("spj,sjk->spk", reach, reach, precision=lax.Precision.HIGHEST), 1.0
        )
    return reach > 0.5


def after_table(count):
    places = jnp.arange(count, dtype=jnp.int32)
    return (places[:, None] > places[None, :]).astype(jnp.float32)


def sum_after(values):
    table = after_table(values.shape[-1])
    return jnp.einsum("shpk,kc->shpc", values, table, precision=lax.Precision.HIGHEST)


def local(
    tokens,
    norm_gain,
    w_query,
    w_key,
    w_value,
    w_gate,
    w_out,
    head_bias,
    cache_keys,
    cache_values,
    prefix_len,
    accepted,
    parent,
):
    seqs, props, columns = tokens.shape
    width = w_query.shape[1]
    heads = width // HEAD
    flat = tokens.astype(jnp.float32).reshape(seqs * props, columns)
    square_part = jnp.sum(flat * flat, axis=1)
    scaled = (flat * norm_gain).astype(jnp.bfloat16)
    partial_value = jnp.concatenate(
        [
            jnp.dot(scaled, weight, preferred_element_type=jnp.float32)
            for weight in (w_query, w_key, w_value, w_gate)
        ],
        axis=1,
    )
    squares = lax.psum(square_part, "kv")
    share = lax.psum_scatter(partial_value, "kv", scatter_dimension=1, tiled=True)
    rscale = lax.rsqrt(squares / D + EPS)
    projected = lax.all_gather(
        (share * rscale[:, None]).astype(jnp.bfloat16), "kv", axis=1, tiled=True
    )
    shaped = projected.reshape(seqs, props, 4, heads, HEAD)
    query = shaped[:, :, 0]
    key_new = shaped[:, :, 1]
    value_new = shaped[:, :, 2]
    gate = projected[:, 3 * width :].astype(jnp.float32)
    factor = HEAD ** (-0.5)
    bias_col = head_bias[None, :, None, None]
    ctx_dev = cache_keys.shape[1]
    places = lax.axis_index("kv") * ctx_dev + jnp.arange(ctx_dev, dtype=jnp.int32)
    valid = prefix_len + accepted
    live = (places[None, :] < valid[:, None])[:, None, None, :]
    scores = (
        jnp.einsum("sphd,schd->shpc", query, cache_keys, preferred_element_type=jnp.float32)
        * factor
        + bias_col
    )
    keep_log = jnp.where(live, jax.nn.log_sigmoid(-scores), 0.0)
    shard_rest = jnp.sum(keep_log, axis=3)
    family = ancestry(parent)[:, None]
    tree_scores = (
        jnp.einsum("sphd,sjhd->shpj", query, key_new, preferred_element_type=jnp.float32) * factor
        + bias_col
    )
    tree_keep = jnp.where(family, jax.nn.log_sigmoid(-tree_scores), 0.0)
    tail = jnp.sum(tree_keep, axis=3)
    every = lax.all_gather(shard_rest[None], "kv", axis=0, tiled=True)
    after = jnp.arange(every.shape[0], dtype=jnp.int32) > lax.axis_index("kv")
    beyond = jnp.sum(jnp.where(after[:, None, None, None], every, 0.0), axis=0)
    later_cache = sum_after(keep_log) + (beyond + tail)[..., None]
    cache_weight = jnp.where(live, jnp.exp(jax.nn.log_sigmoid(scores) + later_cache), 0.0).astype(
        jnp.bfloat16
    )
    later_tree = sum_after(tree_keep)
    tree_weight = jnp.where(
        family, jnp.exp(jax.nn.log_sigmoid(tree_scores) + later_tree), 0.0
    ).astype(jnp.bfloat16)
    local_sum = jnp.einsum(
        "shpc,schd->sphd", cache_weight, cache_values, preferred_element_type=jnp.float32
    )
    attended = lax.psum(local_sum, "kv")
    attended = attended + jnp.einsum(
        "shpj,sjhd->sphd", tree_weight, value_new, preferred_element_type=jnp.float32
    )
    mixin = (attended.reshape(seqs * props, width) * jax.nn.silu(gate)).astype(jnp.bfloat16)
    part_out = jnp.dot(mixin, w_out, preferred_element_type=jnp.float32).astype(jnp.bfloat16)
    part_out = lax.optimization_barrier(part_out).astype(jnp.float32)
    mixed = lax.psum(part_out.astype(jnp.bfloat16), "tp").reshape(seqs, props, w_out.shape[1])
    relative = places[None, :] - valid[:, None]
    picker = (relative[:, :, None] == jnp.arange(props, dtype=jnp.int32)[None, None, :]).astype(
        jnp.bfloat16
    )
    inside = ((relative >= 0) & (relative < props))[:, :, None, None]
    placed_keys = jnp.einsum(
        "scp,sphd->schd", picker, key_new, preferred_element_type=jnp.float32
    ).astype(jnp.bfloat16)
    placed_values = jnp.einsum(
        "scp,sphd->schd", picker, value_new, preferred_element_type=jnp.float32
    ).astype(jnp.bfloat16)
    keys_next = jnp.where(inside, placed_keys, cache_keys)
    values_next = jnp.where(inside, placed_values, cache_values)
    return (mixed, keys_next, values_next)


def solution(mesh):
    return jax.shard_map(
        local,
        mesh=mesh,
        in_specs=(
            P("dp", None, "kv"),
            P("kv"),
            P("kv", "tp"),
            P("kv", "tp"),
            P("kv", "tp"),
            P("kv", "tp"),
            P("tp", "kv"),
            P("tp"),
            P("dp", "kv", "tp", None),
            P("dp", "kv", "tp", None),
            P("dp"),
            P("dp"),
            P("dp", None),
        ),
        out_specs=(P("dp", None, "kv"), P("dp", "kv", "tp", None), P("dp", "kv", "tp", None)),
        check_vma=False,
    )
```

profile of v0, /device:TPU:0, one launch (start us, length us, event | category | flops | bytes accessed | tf_op | source)
XLA Modules:
  0.0 114.4 jit_solution(16729290940814623827)
XLA Ops:
  7.2 0.0 copy-start
  7.2 0.0 reduce-scatter.2.cloned.1.call-start
  7.3 1.3 %copy-done = bf16[512,1536]{1,0:T(8,128)(2,1)S(1)} copy-done((bf16[512,1536]{1,0:T(8,128)(2,1)S(1)}, bf16[512,1536]{1,0:T(8,128)(2,1)}, u32[]{:S(2)}) %copy-start) | copy-done | bytes 1572888
  8.6 1.1 fusion.70
  9.7 0.0 copy-done.4
  9.8 0.0 copy-start.6
  9.8 0.3 fusion.68
  10.1 0.1 copy-done.5
  10.1 0.3 fusion.66
  10.4 0.8 copy-done.6
  11.3 0.3 fusion.64
  11.6 0.8 pad_maximum_fusion
  12.4 0.0 reduce-scatter.2.cloned.1.call-update
  12.4 0.0 all-reduce.2.cloned.1.call-start
  12.4 0.2 fusion.26
  12.6 0.1 fusion.22
  12.8 0.1 fusion.23
  12.9 0.1 fusion.24
  13.0 0.2 fusion.27
  14.5 0.1 copy.29
  14.6 0.1 fusion.52
  14.7 13.6 %psum.21 = f32[16]{0:T(128)S(1)} all-reduce(f32[16]{0:T(128)S(1)} %fusion.52), channel_id=1, replica_groups=mesh['dp'=4,'kv'=4,'tp'=2] {'kv'}, use_global_device_ids=true, to_apply=%region_2.0 | all-reduce | flops 16 | bytes 128 | tf_op jit(solution)/shard_map/psum | solution.py:62
  28.4 7.6 %reduce-scatter.2.cloned.1.call-done = f32[16,1536]{1,0:T(8,128)} async-done(((f32[16,6144]{1,0:T(8,128)}), f32[16,1536]{1,0:T(8,128)}) %reduce-scatter.2.cloned.1.call-update) | async-done | bytes 98320 | tf_op jit(solution)/shard_map/reduce_scatter | solution.py:63
  36.0 1.0 multiply_convert_fusion
  37.0 13.6 %all_gather.6 = bf16[16,6144]{1,0:T(8,128)(2,1)S(1)} all-gather(bf16[16,1536]{1,0:T(8,128)(2,1)S(1)} %multiply_convert_fusion), channel_id=1, replica_groups=mesh['dp'=4,'kv'=4,'tp'=2] {'kv'}, dimensions={1}, use_global_device_ids=true | all-gather | bytes 245760 | tf_op jit(solution)/shard_map/all_gather | solution.py:65
  50.6 0.9 reshape.356
  51.4 0.9 fusion.80
  52.4 0.2 fusion.45
  52.5 0.0 copy-done.1
  52.5 0.0 copy-start.9
  52.6 0.5 fusion.32
  53.1 0.3 fusion.31
  53.4 13.2 %all-gather.1 = f32[4,12,16]{2,1,0:T(8,128)S(1)} all-gather(f32[1,12,16]{2,1,0:T(8,128)S(1)} %bitcast.103), channel_id=2, replica_groups=mesh['dp'=4,'kv'=4,'tp'=2] {'kv'}, dimensions={0}, use_global_device_ids=true | all-gather | bytes 3840 | tf_op jit(solution)/shard_map/all_gather | solution.py:93
  66.6 0.1 fusion.53
  66.6 0.1 fusion.43
  66.7 0.0 copy-start.2
  66.8 0.9 fusion.13
  67.7 0.5 copy-done.2
  68.2 1.0 fusion.14
  69.1 0.0 all-reduce.2.cloned.1.call-update
  69.1 0.0 copy-start.3
  69.2 1.8 %bitcast_select_fusion.1 = bf16[1,512,12,128]{3,1,2,0:T(8,128)(2,1)} fusion(bf16[1,512,12,128]{3,1,2,0:T(8,128)(2,1)S(1)} %copy-done.1, pred[512]{0:T(512)(128)(4,1)S(1)} %compare_and_fusion, bf16[1,16,1,12,128]{4,3,2,1,0:T(8,128)(2,1)S(1)} %get-tuple-element.4, s32[512]{0:T(512)S(1)} %fusion.73), kind=kOutput, calls=%fused_computation.3 | convolution fusion | flops 26746880 | bytes 3197440 | tf_op jit(solution)/shard_map/scp,sphd->schd/dot_general | solution.py:120
  70.9 1.8 %bitcast_select_fusion = bf16[1,512,12,128]{3,1,2,0:T(8,128)(2,1)} fusion(bf16[1,512,12,128]{3,1,2,0:T(8,128)(2,1)S(1)} %copy-done.3, pred[512]{0:T(512)(128)(4,1)S(1)} %compare_and_fusion, bf16[1,16,1,12,128]{4,3,2,1,0:T(8,128)(2,1)S(1)} %get-tuple-element.3, s32[512]{0:T(512)S(1)} %fusion.73), kind=kOutput, calls=%fused_computation.2 | convolution fusion | flops 26746880 | bytes 3197440 | tf_op jit(solution)/shard_map/scp,sphd->schd/dot_general | solution.py:123
  72.7 0.3 fusion.21
  73.0 29.2 %all-reduce.2.cloned.1.call-done = f32[1,16,12,128]{3,1,2,0:T(8,128)} async-done(((f32[1,16,12,128]{3,1,2,0:T(8,128)}), f32[1,16,12,128]{3,1,2,0:T(8,128)}) %all-reduce.2.cloned.1.call-update) | async-done | bytes 98320 | tf_op jit(solution)/shard_map/psum | solution.py:107
  102.2 1.1 fusion.17
  103.3 0.3 convolution_convert_fusion.2
  103.6 4.0 %psum.23 = bf16[1,16,512]{2,1,0:T(8,128)(2,1)} all-reduce(bf16[1,16,512]{2,1,0:T(8,128)(2,1)S(1)} %bitcast.102), channel_id=1, replica_groups=mesh['dp'=4,'kv'=4,'tp'=2] {'tp'}, use_global_device_ids=true, to_apply=%region_7.8 | all-reduce | flops 8192 | bytes 32768 | tf_op jit(solution)/shard_map/psum | solution.py:114
  (24 shorter events, 0.1 us)
Async XLA Ops:
  7.2 1.4 %copy-start = (bf16[512,1536]{1,0:T(8,128)(2,1)S(1)}, bf16[512,1536]{1,0:T(8,128)(2,1)}, u32[]{:S(2)}) copy-start(bf16[512,1536]{1,0:T(8,128)(2,1)} %param.15) | copy-start | bytes 4718596
  7.2 2.5 %copy-start.8 = (bf16[1,16,512]{2,1,0:T(8,128)(2,1)S(1)}, bf16[1,16,512]{2,1,0:T(8,128)(2,1)}, u32[]{:S(2)}) copy-start(bf16[1,16,512]{2,1,0:T(8,128)(2,1)} %param.13) | copy-start | bytes 49156
  7.2 2.5 %copy-start.11 = (f32[512]{0:T(512)S(1)}, f32[512]{0:T(512)}, u32[]{:S(2)}) copy-start(f32[512]{0:T(512)} %param.14) | copy-start | bytes 6148
  7.2 2.5 %copy-start.4 = (bf16[512,1536]{1,0:T(8,128)(2,1)S(1)}, bf16[512,1536]{1,0:T(8,128)(2,1)}, u32[]{:S(2)}) copy-start(bf16[512,1536]{1,0:T(8,128)(2,1)} %param.16) | copy-start | bytes 4718596
  7.2 28.8 %reduce-scatter.2.cloned.1.call-start = ((), (), s32[]{:S(2)}) async-start(), calls=%async_computation.1 | async-start | bytes 491520 | tf_op jit(solution)/shard_map/reduce_scatter | solution.py:63
  8.6 1.6 %copy-start.5 = (bf16[512,1536]{1,0:T(8,128)(2,1)S(1)}, bf16[512,1536]{1,0:T(8,128)(2,1)}, u32[]{:S(2)}) copy-start(bf16[512,1536]{1,0:T(8,128)(2,1)} %param.17) | copy-start | bytes 4718596
  9.8 1.5 %copy-start.6 = (bf16[512,1536]{1,0:T(8,128)(2,1)S(1)}, bf16[512,1536]{1,0:T(8,128)(2,1)}, u32[]{:S(2)}) copy-start(bf16[512,1536]{1,0:T(8,128)(2,1)} %param.18) | copy-start | bytes 4718596
  11.3 1.2 %copy-start.13 = (s32[1,16]{1,0:T(1,128)S(1)}, s32[1,16]{1,0:T(1,128)}, u32[]{:S(2)}) copy-start(s32[1,16]{1,0:T(1,128)} %param.25) | copy-start | bytes 196
  11.6 40.8 %copy-start.12 = (f32[12]{0:T(128)S(1)}, f32[12]{0:T(128)}, u32[]{:S(2)}) copy-start(f32[12]{0:T(128)} %param.20) | copy-start | bytes 148
  11.6 41.0 %copy-start.1 = (bf16[1,512,12,128]{3,1,2,0:T(8,128)(2,1)S(1)}, bf16[1,512,12,128]{3,1,2,0:T(8,128)(2,1)}, u32[]{:S(2)}) copy-start(bf16[1,512,12,128]{3,1,2,0:T(8,128)(2,1)} %param.21) | copy-start | bytes 4718596
  12.4 89.8 %all-reduce.2.cloned.1.call-start = ((), (), s32[]{:S(2)}) async-start(), calls=%async_computation.2 | async-start | bytes 196608 | tf_op jit(solution)/shard_map/psum | solution.py:107
  52.5 15.1 %copy-start.9 = (f32[12,16,16]{1,2,0:T(8,128)}, f32[12,16,16]{1,2,0:T(8,128)S(1)}, u32[]{:S(2)}) copy-start(f32[12,16,16]{1,2,0:T(8,128)S(1)} %get-tuple-element.9) | copy-start | bytes 36868
  66.7 1.4 %copy-start.2 = (bf16[1,512,12,128]{3,1,2,0:T(8,128)(2,1)S(1)}, bf16[1,512,12,128]{3,1,2,0:T(8,128)(2,1)}, u32[]{:S(2)}) copy-start(bf16[1,512,12,128]{3,1,2,0:T(8,128)(2,1)} %param.22) | copy-start | bytes 4718596
  69.1 1.8 %copy-start.3 = (bf16[1,512,12,128]{3,1,2,0:T(8,128)(2,1)S(1)}, bf16[1,512,12,128]{3,1,2,0:T(8,128)(2,1)}, u32[]{:S(2)}) copy-start(bf16[1,512,12,128]{3,1,2,0:T(8,128)(2,1)} %param.22) | copy-start | bytes 4718596
  70.9 1.8 %copy-start.10 = (f32[12,16,16]{1,2,0:T(8,128)S(1)}, f32[12,16,16]{1,2,0:T(8,128)}, u32[]{:S(2)}) copy-start(f32[12,16,16]{1,2,0:T(8,128)} %copy-done.9) | copy-start | bytes 36868
  70.9 32.4 %copy-start.7 = (bf16[1536,512]{1,0:T(8,128)(2,1)S(1)}, bf16[1536,512]{1,0:T(8,128)(2,1)}, u32[]{:S(2)}) copy-start(bf16[1536,512]{1,0:T(8,128)(2,1)} %param.19) | copy-start | bytes 4718596
Sparse Core Ops, SparseCore 0:
  12.5 23.4 reduce-scatter.1
  69.3 32.8 all-reduce.1
where the time goes:
time: 115 us; the launch traced here: 114 us
  blocking collectives  44.4 us (39%)
  waiting for transfers between devices  36.8 us (32%)
  between operations  15.5 us (13%)
  matrix products  10.6 us (9%)
  local copies, waits for them, and re-layouts  4.63 us (4%)
  other arithmetic  2.38 us (2%)
    psum x1, waiting for transfers between devices, local(): attended = lax.psum(local_sum, 'kv')  29.2 us
    psum x1, blocking collectives, local(): squares = lax.psum(square_part, 'kv')  13.6 us
    all_gather x1, blocking collectives, local(): lax.all_gather((share * rscale[:, None]).astype(jnp.bfloat16), 'kv', axis...  13.6 us
    all_gather x1, blocking collectives, local(): every = lax.all_gather(shard_rest[None], 'kv', axis=0, tiled=True)  13.2 us
    reduce_scatter x1, waiting for transfers between devices, local(): lax.psum_scatter(partial_value, 'kv', scatter_dimension=1, tiled=True)  7.6 us
    psum x1, blocking collectives, local(): lax.psum(part_out.astype(jnp.bfloat16), 'tp')  3.96 us
    unnamed x28, local copies, waits for them, and re-layouts  2.74 us
  transfers between devices with their start and end apart: 2, of which 2 were waited for; matrix products, arithmetic and copies ran while one was open for 4% of the time, Pallas kernels for 0%

commit v1 on v0

--- a/solution.py
+++ b/solution.py
@@ -1,10 +1,16 @@
+import functools
+
 import jax
 import jax.numpy as jnp
 from jax import lax
+from jax.experimental import pallas as pl
+from jax.experimental.pallas import tpu as pltpu
 from jax.sharding import PartitionSpec as P
 
 D = 2048
 HEAD = 128
+LANES = 128
+MESH = pl.DeviceIdType.MESH
 
 
 EPS = 1e-06
@@ -128,9 +134,564 @@
     return (mixed, keys_next, values_next)
 
 
+def softplus_tail(scores):
+    return jnp.log1p(jnp.exp(-jnp.abs(scores)))
+
+
+def three_parts(values):
+    high = values.astype(jnp.bfloat16).astype(jnp.float32)
+    rest = values - high
+    middle = rest.astype(jnp.bfloat16).astype(jnp.float32)
+    return high, middle, rest - middle
+
+
+def lanes_of(columns, props):
+    lane = lax.broadcasted_iota(jnp.int32, (props, LANES), 1)
+    block = jnp.zeros((props, LANES), jnp.float32)
+    for place, column in enumerate(columns):
+        block = block + jnp.where(lane == place, column, 0.0)
+    return block.astype(jnp.bfloat16)
+
+
+def exchange_kernel(
+    n_kv,
+    first_writer,
+    tokens_ref,
+    gain_ref,
+    wq_hbm,
+    wk_hbm,
+    wv_hbm,
+    wg_hbm,
+    wo_hbm,
+    bias_ref,
+    keys_hbm,
+    values_hbm,
+    prefix_ref,
+    accepted_ref,
+    parent_ref,
+    parts_ref,
+    fresh_ref,
+    w_in,
+    w_out,
+    keys,
+    values,
+    partial,
+    table,
+    q_send,
+    q_recv,
+    q_own,
+    q_all,
+    p_send,
+    p_recv,
+    s_send,
+    s_recv,
+    m_send,
+    m_recv,
+    f_send,
+    f_recv,
+    o_recv,
+    o_send,
+    local_sem,
+    send_sem,
+    recv_sem,
+):
+    me = lax.axis_index("kv")
+    core = lax.axis_index("tp")
+    props, columns = tokens_ref.shape
+    heads, ctx, head = keys.shape
+    own = heads // n_kv
+    group = own * head
+    peers = [lax.rem(me + step, n_kv) for step in range(n_kv)]
+    sources = [lax.rem(me + n_kv - step, n_kv) for step in range(n_kv)]
+
+    barrier = pltpu.get_barrier_semaphore()
+    for step in range(1, n_kv):
+        pl.semaphore_signal(
+            barrier, inc=1, device_id={"kv": peers[step]}, device_id_type=MESH
+        )
+    pl.semaphore_signal(barrier, inc=1, device_id={"tp": 1 - core}, device_id_type=MESH)
+
+    loads = []
+    for place, (src, dst) in enumerate(
+        [
+            (wq_hbm, w_in.at[0]),
+            (wk_hbm, w_in.at[1]),
+            (wv_hbm, w_in.at[2]),
+            (wg_hbm, w_in.at[3]),
+            (keys_hbm, keys),
+            (values_hbm, values),
+            (wo_hbm, w_out),
+        ]
+    ):
+        copy = pltpu.make_async_copy(src, dst, local_sem.at[place])
+        copy.start()
+        loads.append(copy)
+
+    started = []
+
+    def send(kind, step, src, dst, device):
+        copy = pltpu.make_async_remote_copy(
+            src_ref=src,
+            dst_ref=dst,
+            send_sem=send_sem.at[kind, step],
+            recv_sem=recv_sem.at[kind, step],
+            device_id=device,
+            device_id_type=MESH,
+        )
+        copy.start()
+        return copy
+
+    flat = tokens_ref[...].astype(jnp.float32)
+    square_part = jnp.sum(flat * flat, axis=1, keepdims=True)
+    scaled = (flat * gain_ref[...]).astype(jnp.bfloat16)
+    square_lanes = lanes_of(three_parts(square_part), props)
+    for owner in range(n_kv):
+        q_send[owner, :, group:] = square_lanes
+
+    def project(which):
+        loads[which].wait()
+        return jnp.dot(scaled, w_in[which], preferred_element_type=jnp.float32)
+
+    part = project(0)
+    for owner in range(n_kv):
+        block = part[:, owner * group : (owner + 1) * group]
+        partial[owner, :, :group] = block
+        q_send[owner, :, :group] = block.astype(jnp.bfloat16)
+    pl.semaphore_wait(barrier, n_kv)
+    q_copies = [
+        send(0, step, q_send.at[peers[step]], q_recv.at[step], {"kv": peers[step]})
+        for step in range(n_kv - 1, 0, -1)
+    ]
+    started += q_copies
+
+    for which in range(1, 4):
+        part = project(which)
+        for owner in range(n_kv):
+            block = part[:, owner * group : (owner + 1) * group]
+            partial[owner, :, which * group : (which + 1) * group] = block
+            p_send[owner, :, (which - 1) * group : which * group] = block.astype(jnp.bfloat16)
+    rows = lax.broadcasted_iota(jnp.int32, (ctx, ctx), 0)
+    cols = lax.broadcasted_iota(jnp.int32, (ctx, ctx), 1)
+    table[...] = jnp.where(rows > cols, 1.0, 0.0).astype(jnp.bfloat16)
+
+    place_p = lax.broadcasted_iota(jnp.int32, (props, props), 0)
+    place_j = lax.broadcasted_iota(jnp.int32, (props, props), 1)
+    reach = jnp.where(parent_ref[...] == place_p, 1.0, 0.0)
+    for repeat in range(props.bit_length()):
+        reach = jnp.minimum(
+            reach + jnp.dot(reach, reach, preferred_element_type=jnp.float32), 1.0
+        )
+    unit = jnp.where(place_p == place_j, 1.0, 0.0)
+    reach = lax.dot_general(
+        reach, unit, (((0,), (0,)), ((), ())), preferred_element_type=jnp.float32
+    )
+    family = jnp.concatenate([reach] * own, axis=0) > 0.5
+    tree_table = jnp.where(place_p > place_j, 1.0, 0.0)
+
+    total = partial[me, :, :group]
+    squares = square_part
+    for copy, step in zip(q_copies, range(n_kv - 1, 0, -1)):
+        copy.wait_recv()
+        total = total + q_recv[step, :, :group].astype(jnp.float32)
+        lanes = q_recv[step, :, group:].astype(jnp.float32)
+        squares = squares + (lanes[:, 0:1] + lanes[:, 1:2] + lanes[:, 2:3])
+    rscale = lax.rsqrt(squares / (columns * n_kv) + EPS)
+    q_mine = (total * rscale).astype(jnp.bfloat16)
+    q_own[...] = q_mine
+    a_copies = [
+        send(1, step, q_own, q_all.at[step], {"kv": peers[step]})
+        for step in range(n_kv - 1, 0, -1)
+    ][::-1]
+    started += a_copies
+    p_copies = [
+        send(2, step, p_send.at[peers[step]], p_recv.at[step], {"kv": peers[step]})
+        for step in range(n_kv - 1, 0, -1)
+    ]
+    started += p_copies
+
+    factor = head ** (-0.5)
+    valid = prefix_ref[0] + accepted_ref[0]
+    live = lax.broadcasted_iota(jnp.int32, (own * props, ctx), 1) + me * ctx < valid
+
+    def attend(step):
+        owner = sources[step]
+        query = q_mine if step == 0 else q_all[step]
+        scores = jnp.concatenate(
+            [
+                lax.dot_general(
+                    query[:, each * head : (each + 1) * head],
+                    keys[owner * own + each],
+                    (((1,), (1,)), ((), ())),
+                    preferred_element_type=jnp.float32,
+                )
+                * factor
+                + bias_ref[owner * own + each]
+                for each in range(own)
+            ],
+            axis=0,
+        )
+        soft = softplus_tail(scores)
+        keep = jnp.where(live, -(jnp.maximum(scores, 0.0) + soft), 0.0)
+        rest = jnp.sum(keep, axis=1, keepdims=True)
+        high = keep.astype(jnp.bfloat16)
+        low = (keep - high.astype(jnp.float32)).astype(jnp.bfloat16)
+        later = jnp.dot(high, table[...], preferred_element_type=jnp.float32) + jnp.dot(
+            low, table[...], preferred_element_type=jnp.float32
+        )
+        weight = jnp.where(live, jnp.exp(jnp.minimum(scores, 0.0) - soft + later), 0.0).astype(
+            jnp.bfloat16
+        )
+        if step == 0:
+            loads[5].wait()
+        sums = [
+            jnp.dot(
+                weight[each * props : (each + 1) * props],
+                values[owner * own + each],
+                preferred_element_type=jnp.float32,
+            )
+            for each in range(own)
+        ]
+        rests = [rest[each * props : (each + 1) * props] for each in range(own)]
+        return sums, rests
+
+    loads[4].wait()
+    sums_by, rests_by = [None] * n_kv, [None] * n_kv
+    sums_by[0], rests_by[0] = attend(0)
+    s_copies = [None] * n_kv
+    for step in range(1, n_kv):
+        a_copies[step - 1].wait_recv()
+        sums, rests = attend(step)
+        for each in range(own):
+            s_send[step, :, each * head : (each + 1) * head] = sums[each].astype(jnp.bfloat16)
+        pieces = [three_parts(rest) for rest in rests]
+        s_send[step, :, group:] = lanes_of(
+            [piece[level] for level in range(3) for piece in pieces], props
+        )
+        s_copies[step] = send(
+            3, step, s_send.at[step], s_recv.at[step], {"kv": sources[step]}
+        )
+        started.append(s_copies[step])
+
+    fresh = partial[me, :, group:]
+    for copy, step in zip(p_copies, range(n_kv - 1, 0, -1)):
+        copy.wait_recv()
+        fresh = fresh + p_recv[step].astype(jnp.float32)
+    fresh = (fresh * rscale).astype(jnp.bfloat16)
+    key_new = fresh[:, :group]
+    value_new = fresh[:, group : 2 * group]
+    gate = fresh[:, 2 * group :].astype(jnp.float32)
+    f_send[...] = fresh[:, : 2 * group]
+    fresh_ref[...] = jnp.zeros_like(fresh_ref)
+    fresh_ref[me] = fresh[:, : 2 * group]
+
+    tree_scores = jnp.concatenate(
+        [
+            lax.dot_general(
+                q_mine[:, each * head : (each + 1) * head],
+                key_new[:, each * head : (each + 1) * head],
+                (((1,), (1,)), ((), ())),
+                preferred_element_type=jnp.float32,
+            )
+            * factor
+            + bias_ref[me * own + each]
+            for each in range(own)
+        ],
+        axis=0,
+    )
+    soft = softplus_tail(tree_scores)
+    tree_keep = jnp.where(family, -(jnp.maximum(tree_scores, 0.0) + soft), 0.0)
+    tail = jnp.sum(tree_keep, axis=1, keepdims=True)
+    later = jnp.dot(
+        tree_keep,
+        tree_table,
+        precision=lax.Precision.HIGHEST,
+        preferred_element_type=jnp.float32,
+    )
+    tree_weight = jnp.where(
+        family, jnp.exp(jnp.minimum(tree_scores, 0.0) - soft + later), 0.0
+    ).astype(jnp.bfloat16)
+    tree_sums = [
+        jnp.dot(
+            tree_weight[each * props : (each + 1) * props],
+            value_new[:, each * head : (each + 1) * head],
+            preferred_element_type=jnp.float32,
+        )
+        for each in range(own)
+    ]
+    silu = gate / (1.0 + jnp.exp(-gate))
+
+    for step in range(1, n_kv):
+        s_copies[step].wait_recv()
+        lanes = s_recv[step, :, group:].astype(jnp.float32)
+        rests_by[step] = [
+            lanes[:, each : each + 1]
+            + lanes[:, own + each : own + each + 1]
+            + lanes[:, 2 * own + each : 2 * own + each + 1]
+            for each in range(own)
+        ]
+        sums_by[step] = [
+            s_recv[step, :, each * head : (each + 1) * head].astype(jnp.float32)
+            for each in range(own)
+        ]
+    for each in range(own):
+        attended = tree_sums[each]
+        for step in range(n_kv):
+            beyond = tail[each * props : (each + 1) * props]
+            for other in range(n_kv):
+                if other != step:
+                    after = jnp.where(peers[other] > peers[step], 1.0, 0.0)
+                    beyond = beyond + rests_by[other][each] * after
+            attended = attended + jnp.exp(beyond) * sums_by[step][each]
+        m_send[:, each * head : (each + 1) * head] = (
+            attended * silu[:, each * head : (each + 1) * head]
+        ).astype(jnp.bfloat16)
+    m_copies = [
+        send(4, step, m_send, m_recv.at[step], {"kv": peers[step]})
+        for step in range(n_kv - 1, 0, -1)
+    ][::-1]
+    started += m_copies
+
+    def hand(step):
+        return pltpu.make_async_remote_copy(
+            src_ref=f_send,
+            dst_ref=f_recv.at[step],
+            send_sem=send_sem.at[5, step],
+            recv_sem=recv_sem.at[5, step],
+            device_id={"kv": peers[step]},
+            device_id_type=MESH,
+        )
+
+    for step in range(1, n_kv):
+
+        @pl.when(peers[step] >= first_writer)
+        def _(step=step):
+            hand(step).start()
+
+    loads[6].wait()
+
+    def out_rows(step):
+        start = pl.multiple_of(sources[step] * group, group)
+        return w_out[pl.ds(start, group), :]
+
+    mixed = jnp.dot(m_send[...], out_rows(0), preferred_element_type=jnp.float32)
+    for step in range(1, n_kv):
+        m_copies[step - 1].wait_recv()
+        mixed = mixed + jnp.dot(
+            m_recv[step], out_rows(step), preferred_element_type=jnp.float32
+        )
+    mixed = mixed.astype(jnp.bfloat16)
+    o_send[...] = mixed
+    o_copy = send(6, 0, o_send, o_recv, {"tp": 1 - core})
+    parts_ref[0] = mixed
+
+    @pl.when(me >= first_writer)
+    def _():
+        for step in range(1, n_kv):
+            hand(step).wait_recv()
+            fresh_ref[sources[step]] = f_recv[step]
+
+    for copy in started:
+        copy.wait_send()
+    for step in range(1, n_kv):
+
+        @pl.when(peers[step] >= first_writer)
+        def _(step=step):
+            hand(step).wait_send()
+
+    o_copy.wait()
+    parts_ref[1] = o_recv[...]
+
+
+CHUNKS = 4
+
+
+def cache_kernel(
+    parts_ref,
+    fresh_ref,
+    prefix_ref,
+    accepted_ref,
+    keys_hbm,
+    values_hbm,
+    mixed_ref,
+    keys_out,
+    values_out,
+    keys,
+    values,
+    in_sem,
+    out_sem,
+):
+    heads, ctx, head = keys.shape
+    n_kv, props, wide = fresh_ref.shape
+    own = heads // n_kv
+    step_heads = heads // CHUNKS
+    pairs = []
+    for chunk in range(CHUNKS):
+        span = pl.ds(chunk * step_heads, step_heads)
+        for side, (src, held, dst) in enumerate(
+            [(keys_hbm, keys, keys_out), (values_hbm, values, values_out)]
+        ):
+            copy = pltpu.make_async_copy(
+                src.at[span], held.at[span], in_sem.at[chunk, side]
+            )
+            copy.start()
+            back = pltpu.make_async_copy(
+                held.at[span], dst.at[span], out_sem.at[chunk, side]
+            )
+            pairs.append((chunk, side, held, copy, back))
+    mixed_ref[...] = (
+        parts_ref[0].astype(jnp.float32) + parts_ref[1].astype(jnp.float32)
+    ).astype(jnp.bfloat16)
+    start = prefix_ref[0] + accepted_ref[0] - lax.axis_index("kv") * ctx
+    window = 2 * props
+    base = pl.multiple_of(jnp.clip(start // props, 0, ctx // props - 2) * props, props)
+    touched = (start + props > 0) & (start < ctx)
+    row = lax.broadcasted_iota(jnp.int32, (window, props), 0) + base - start
+    column = lax.broadcasted_iota(jnp.int32, (window, props), 1)
+    picker = jnp.where(row == column, 1.0, 0.0).astype(jnp.bfloat16)
+    offset = lax.broadcasted_iota(jnp.int32, (window, head), 0) + base - start
+    inside = (offset >= 0) & (offset < props)
+    for chunk, side, held, copy, back in pairs:
+        copy.wait()
+
+        @pl.when(touched)
+        def _(chunk=chunk, side=side, held=held):
+            for place in range(chunk * step_heads, (chunk + 1) * step_heads):
+                at = side * own * head + (place % own) * head
+                placed = jnp.dot(
+                    picker,
+                    fresh_ref[place // own, :, at : at + head],
+                    preferred_element_type=jnp.float32,
+                )
+                now = held[place, pl.ds(base, window), :].astype(jnp.float32)
+                held[place, pl.ds(base, window), :] = jnp.where(inside, placed, now).astype(
+                    jnp.bfloat16
+                )
+
+        back.start()
+    for chunk, side, held, copy, back in pairs:
+        back.wait()
+
+
+def fast(
+    n_kv,
+    tokens,
+    norm_gain,
+    w_query,
+    w_key,
+    w_value,
+    w_gate,
+    w_out,
+    head_bias,
+    cache_keys,
+    cache_values,
+    prefix_len,
+    accepted,
+    parent,
+):
+    _, props, columns = tokens.shape
+    width = w_query.shape[1]
+    heads = width // HEAD
+    ctx = cache_keys.shape[1]
+    out_columns = w_out.shape[1]
+    group = width // n_kv
+    whole = ctx * n_kv
+    first_writer = (whole - whole // 4) // ctx
+    keys = jnp.transpose(cache_keys[0], (1, 0, 2))
+    values = jnp.transpose(cache_values[0], (1, 0, 2))
+    vmem = pl.BlockSpec(memory_space=pltpu.VMEM)
+    smem = pl.BlockSpec(memory_space=pltpu.SMEM)
+    hbm = pl.BlockSpec(memory_space=pl.ANY)
+    low = jnp.bfloat16
+    cache_shape = (heads, ctx, HEAD)
+    parts, fresh = pl.pallas_call(
+        functools.partial(exchange_kernel, n_kv, first_writer),
+        out_shape=(
+            jax.ShapeDtypeStruct((2, props, out_columns), low),
+            jax.ShapeDtypeStruct((n_kv, props, 2 * group), low),
+        ),
+        in_specs=[vmem, vmem, hbm, hbm, hbm, hbm, hbm, smem, hbm, hbm, smem, smem, vmem],
+        out_specs=(vmem, vmem),
+        scratch_shapes=[
+            pltpu.VMEM((4, columns, width), low),
+            pltpu.VMEM((width, out_columns), low),
+            pltpu.VMEM(cache_shape, low),
+            pltpu.VMEM(cache_shape, low),
+            pltpu.VMEM((n_kv, props, 4 * group), jnp.float32),
+            pltpu.VMEM((ctx, ctx), low),
+            pltpu.VMEM((n_kv, props, group + LANES), low),
+            pltpu.VMEM((n_kv, props, group + LANES), low),
+            pltpu.VMEM((props, group), low),
+            pltpu.VMEM((n_kv, props, group), low),
+            pltpu.VMEM((n_kv, props, 3 * group), low),
+            pltpu.VMEM((n_kv, props, 3 * group), low),
+            pltpu.VMEM((n_kv, props, group + LANES), low),
+            pltpu.VMEM((n_kv, props, group + LANES), low),
+            pltpu.VMEM((props, group), low),
+            pltpu.VMEM((n_kv, props, group), low),
+            pltpu.VMEM((props, 2 * group), low),
+            pltpu.VMEM((n_kv, props, 2 * group), low),
+            pltpu.VMEM((props, out_columns), low),
+            pltpu.VMEM((props, out_columns), low),
+            pltpu.SemaphoreType.DMA((7,)),
+            pltpu.SemaphoreType.DMA((7, n_kv)),
+            pltpu.SemaphoreType.DMA((7, n_kv)),
+        ],
+        compiler_params=pltpu.CompilerParams(
+            collective_id=0, has_side_effects=True, vmem_limit_bytes=40 * 1024 * 1024
+        ),
+        name="exchange",
+    )(
+        tokens[0],
+        norm_gain[None],
+        w_query,
+        w_key,
+        w_value,
+        w_gate,
+        w_out,
+        head_bias,
+        keys,
+        values,
+        prefix_len,
+        accepted,
+        parent,
+    )
+    mixed, keys_next, values_next = pl.pallas_call(
+        cache_kernel,
+        out_shape=(
+            jax.ShapeDtypeStruct((props, out_columns), low),
+            jax.ShapeDtypeStruct(cache_shape, low),
+            jax.ShapeDtypeStruct(cache_shape, low),
+        ),
+        in_specs=[vmem, vmem, smem, smem, hbm, hbm],
+        out_specs=(vmem, hbm, hbm),
+        scratch_shapes=[
+            pltpu.VMEM(cache_shape, low),
+            pltpu.VMEM(cache_shape, low),
+            pltpu.SemaphoreType.DMA((CHUNKS, 2)),
+            pltpu.SemaphoreType.DMA((CHUNKS, 2)),
+        ],
+        compiler_params=pltpu.CompilerParams(vmem_limit_bytes=16 * 1024 * 1024),
+        name="cache",
+    )(parts, fresh, prefix_len, accepted, keys, values)
+    return (
+        mixed[None],
+        jnp.transpose(keys_next, (1, 0, 2))[None],
+        jnp.transpose(values_next, (1, 0, 2))[None],
+    )
+
+
 def solution(mesh):
+    n_kv, n_tp = mesh.shape["kv"], mesh.shape["tp"]
+
+    def body(*arrays):
+        seqs, heads, ctx = arrays[0].shape[0], arrays[8].shape[2], arrays[8].shape[1]
+        fits = heads % n_kv == 0 and heads % CHUNKS == 0 and seqs == 1 and n_tp == 2
+        if fits and n_kv % 4 == 0 and ctx % 128 == 0:
+            return fast(n_kv, *arrays)
+        return local(*arrays)
+
     return jax.shard_map(
-        local,
+        body,
         mesh=mesh,
         in_specs=(
             P("dp", None, "kv"),

time: 115 us -> 42.9 us (0.37)
  blocking collectives: 44.4 us -> 0 us
  waiting for transfers between devices: 36.8 us -> 0 us
  Pallas kernels: 0 us -> 27.9 us
  between operations: 15.5 us -> 1.95 us
  matrix products: 10.6 us -> 0 us
  local copies, waits for them, and re-layouts: 4.63 us -> 12.6 us
  other arithmetic: 2.38 us -> 0 us
    psum x1 -> x0, waiting for transfers between devices: 29.2 us -> none  [local(): attended = lax.psum(local_sum, 'kv')]
    pallas_call x0 -> x2, Pallas kernels: none -> 27.9 us  [the longest x1 24 us: fast(): pl.pallas_call(functools.partial(exchange_kernel, n_kv, first_writer), ou...]
    all_gather x2 -> x0, blocking collectives: 26.8 us -> none  [the longest x1 13.6 us: local(): lax.all_gather((share * rscale[:, None]).astype(jnp.bfloat16), 'kv', axis...]
    psum x2 -> x0, blocking collectives: 17.6 us -> none  [the longest x1 13.6 us: local(): squares = lax.psum(square_part, 'kv')]
    dot_general x18 -> x0, matrix products: 10.6 us -> none  [the longest x4 2.06 us: local(): jnp.dot(scaled, weight, preferred_element_type=jnp.float32)]
    unnamed x28 -> x22, local copies, waits for them, and re-layouts: 2.74 us -> 12.6 us
    reduce_scatter x1 -> x0, waiting for transfers between devices: 7.6 us -> none  [local(): lax.psum_scatter(partial_value, 'kv', scatter_dimension=1, tiled=True)]
  transfers between devices with their start and end apart: 2 -> 0, of which waited for: 2 -> 0; matrix products, arithmetic and copies ran while one was open for 4% -> 0% of each run, Pallas kernels for 0% -> 0%
where the time goes in v1:
time: 42.9 us; the launch traced here: 42.4 us
  Pallas kernels  27.9 us (65%)
  local copies, waits for them, and re-layouts  12.6 us (29%)
  between operations  1.95 us (5%)
    pallas_call x1, Pallas kernels, fast(): pl.pallas_call(functools.partial(exchange_kernel, n_kv, first_writer), ou...  24 us
    unnamed x22, local copies, waits for them, and re-layouts  12.6 us
    pallas_call x1, Pallas kernels, fast(): pl.pallas_call(cache_kernel, out_shape=(jax.ShapeDtypeStruct((props, out_...  3.92 us

profile of v1, /device:TPU:0, one launch (start us, length us, event | category | flops | bytes accessed | tf_op | source)
XLA Modules:
  0.0 42.4 jit_solution(699793324534157350)
XLA Ops:
  1.9 0.0 copy-start
  1.9 1.4 %copy-done = bf16[1,512,12,128]{3,1,2,0:T(8,128)(2,1)S(1)} copy-done((bf16[1,512,12,128]{3,1,2,0:T(8,128)(2,1)S(1)}, bf16[1,512,12,128]{3,1,2,0:T(8,128)(2,1)}, u32[]{:S(2)}) %copy-start) | copy-done | bytes 1572888
  3.3 0.0 copy-start.1
  3.3 1.4 %copy-done.1 = bf16[1,512,12,128]{3,1,2,0:T(8,128)(2,1)S(1)} copy-done((bf16[1,512,12,128]{3,1,2,0:T(8,128)(2,1)S(1)}, bf16[1,512,12,128]{3,1,2,0:T(8,128)(2,1)}, u32[]{:S(2)}) %copy-start.1) | copy-done | bytes 1572888
  4.7 0.0 copy-start.2
  4.7 1.4 %copy-done.2 = bf16[512,1536]{1,0:T(8,128)(2,1)S(1)} copy-done((bf16[512,1536]{1,0:T(8,128)(2,1)S(1)}, bf16[512,1536]{1,0:T(8,128)(2,1)}, u32[]{:S(2)}) %copy-start.2) | copy-done | bytes 1572888
  6.2 0.0 copy-start.3
  6.2 1.4 %copy-done.3 = bf16[512,1536]{1,0:T(8,128)(2,1)S(1)} copy-done((bf16[512,1536]{1,0:T(8,128)(2,1)S(1)}, bf16[512,1536]{1,0:T(8,128)(2,1)}, u32[]{:S(2)}) %copy-start.3) | copy-done | bytes 1572888
  7.6 0.0 copy-start.4
  7.6 1.4 %copy-done.4 = bf16[512,1536]{1,0:T(8,128)(2,1)S(1)} copy-done((bf16[512,1536]{1,0:T(8,128)(2,1)S(1)}, bf16[512,1536]{1,0:T(8,128)(2,1)}, u32[]{:S(2)}) %copy-start.4) | copy-done | bytes 1572888
  9.0 0.0 copy-start.5
  9.0 1.4 %copy-done.5 = bf16[512,1536]{1,0:T(8,128)(2,1)S(1)} copy-done((bf16[512,1536]{1,0:T(8,128)(2,1)S(1)}, bf16[512,1536]{1,0:T(8,128)(2,1)}, u32[]{:S(2)}) %copy-start.5) | copy-done | bytes 1572888
  10.4 0.0 copy-start.6
  10.4 1.4 %copy-done.6 = bf16[1536,512]{1,0:T(8,128)(2,1)S(1)} copy-done((bf16[1536,512]{1,0:T(8,128)(2,1)S(1)}, bf16[1536,512]{1,0:T(8,128)(2,1)}, u32[]{:S(2)}) %copy-start.6) | copy-done | bytes 1572888
  11.8 0.0 copy-start.7
  11.8 0.7 %copy-done.7 = bf16[1,16,512]{2,1,0:T(8,128)(2,1)S(1)} copy-done((bf16[1,16,512]{2,1,0:T(8,128)(2,1)S(1)}, bf16[1,16,512]{2,1,0:T(8,128)(2,1)}, u32[]{:S(2)}) %copy-start.7) | copy-done | bytes 16408
  12.5 0.0 copy-start.8
  12.5 0.7 %copy-done.8 = f32[512]{0:T(512)S(1)} copy-done((f32[512]{0:T(512)S(1)}, f32[512]{0:T(512)}, u32[]{:S(2)}) %copy-start.8) | copy-done | bytes 2072
  13.2 0.0 copy-start.9
  13.2 0.7 %copy-done.9 = f32[12]{0:T(128)S(1)} copy-done((f32[12]{0:T(128)S(1)}, f32[12]{0:T(128)}, u32[]{:S(2)}) %copy-start.9) | copy-done | bytes 72
  13.8 0.0 copy-start.10
  13.8 0.7 %copy-done.10 = s32[1,16]{1,0:T(1,128)S(1)} copy-done((s32[1,16]{1,0:T(1,128)S(1)}, s32[1,16]{1,0:T(1,128)}, u32[]{:S(2)}) %copy-start.10) | copy-done | bytes 88
  14.5 24.0 %exchange.1 = (bf16[2,16,512]{2,1,0:T(8,128)(2,1)S(1)}, bf16[4,16,768]{2,1,0:T(8,128)(2,1)S(1)}) custom-call(bf16[16,512]{1,0:T(8,128)(2,1)S(1)} %bitcast.19, f32[1,512]{1,0:T(1,128)S(1)} %bitcast.20, bf16[512,1536]{1,0:T(8,128)(2,1)S(1)} %copy-done.2, bf16[512,1536]{1,0:T(8,128)(2,1)S(1)} %copy-done.3, bf16[512,1536]{1,0:T(8,128)(2,1)S(1)} %copy-done.4, ...), custom_call_target="tpu_custom_call" | custom-call | tf_op jit(solution)/shard_map/exchange/pallas_call | solution.py:606
  38.5 3.9 %cache.1 = (bf16[16,512]{1,0:T(8,128)(2,1)}, bf16[12,512,128]{2,1,0:T(8,128)(2,1)}, bf16[12,512,128]{2,1,0:T(8,128)(2,1)}) custom-call(bf16[2,16,512]{2,1,0:T(8,128)(2,1)S(1)} %get-tuple-element.8.parts_ref, bf16[4,16,768]{2,1,0:T(8,128)(2,1)S(1)} %get-tuple-element.9.fresh_ref, s32[1]{0:T(128)S(6)} %copy.16.prefix_ref, s32[1]{0:T(128)S(6)} %copy.17.accepted_ref, ...), custom_call_target="tpu_custom_call" | custom-call | tf_op jit(solution)/shard_map/cache/pallas_call | solution.py:658
Async XLA Ops:
  1.9 1.4 %copy-start = (bf16[1,512,12,128]{3,1,2,0:T(8,128)(2,1)S(1)}, bf16[1,512,12,128]{3,1,2,0:T(8,128)(2,1)}, u32[]{:S(2)}) copy-start(bf16[1,512,12,128]{3,1,2,0:T(8,128)(2,1)} %param.21) | copy-start | bytes 4718596
  3.3 1.4 %copy-start.1 = (bf16[1,512,12,128]{3,1,2,0:T(8,128)(2,1)S(1)}, bf16[1,512,12,128]{3,1,2,0:T(8,128)(2,1)}, u32[]{:S(2)}) copy-start(bf16[1,512,12,128]{3,1,2,0:T(8,128)(2,1)} %param.22) | copy-start | bytes 4718596
  4.7 1.4 %copy-start.2 = (bf16[512,1536]{1,0:T(8,128)(2,1)S(1)}, bf16[512,1536]{1,0:T(8,128)(2,1)}, u32[]{:S(2)}) copy-start(bf16[512,1536]{1,0:T(8,128)(2,1)} %wq_hbm.1) | copy-start | bytes 4718596
  6.2 1.4 %copy-start.3 = (bf16[512,1536]{1,0:T(8,128)(2,1)S(1)}, bf16[512,1536]{1,0:T(8,128)(2,1)}, u32[]{:S(2)}) copy-start(bf16[512,1536]{1,0:T(8,128)(2,1)} %wk_hbm.1) | copy-start | bytes 4718596
  7.6 1.4 %copy-start.4 = (bf16[512,1536]{1,0:T(8,128)(2,1)S(1)}, bf16[512,1536]{1,0:T(8,128)(2,1)}, u32[]{:S(2)}) copy-start(bf16[512,1536]{1,0:T(8,128)(2,1)} %wv_hbm.1) | copy-start | bytes 4718596
  9.0 1.4 %copy-start.5 = (bf16[512,1536]{1,0:T(8,128)(2,1)S(1)}, bf16[512,1536]{1,0:T(8,128)(2,1)}, u32[]{:S(2)}) copy-start(bf16[512,1536]{1,0:T(8,128)(2,1)} %wg_hbm.1) | copy-start | bytes 4718596
  10.4 1.4 %copy-start.6 = (bf16[1536,512]{1,0:T(8,128)(2,1)S(1)}, bf16[1536,512]{1,0:T(8,128)(2,1)}, u32[]{:S(2)}) copy-start(bf16[1536,512]{1,0:T(8,128)(2,1)} %wo_hbm.1) | copy-start | bytes 4718596
  11.8 0.7 %copy-start.7 = (bf16[1,16,512]{2,1,0:T(8,128)(2,1)S(1)}, bf16[1,16,512]{2,1,0:T(8,128)(2,1)}, u32[]{:S(2)}) copy-start(bf16[1,16,512]{2,1,0:T(8,128)(2,1)} %param.13) | copy-start | bytes 49156
  12.5 0.7 %copy-start.8 = (f32[512]{0:T(512)S(1)}, f32[512]{0:T(512)}, u32[]{:S(2)}) copy-start(f32[512]{0:T(512)} %param.14) | copy-start | bytes 6148
  13.2 0.7 %copy-start.9 = (f32[12]{0:T(128)S(1)}, f32[12]{0:T(128)}, u32[]{:S(2)}) copy-start(f32[12]{0:T(128)} %bias_ref.1) | copy-start | bytes 148
  13.8 0.7 %copy-start.10 = (s32[1,16]{1,0:T(1,128)S(1)}, s32[1,16]{1,0:T(1,128)}, u32[]{:S(2)}) copy-start(s32[1,16]{1,0:T(1,128)} %parent_ref.1) | copy-start | bytes 196

commit v2 on v1

--- a/solution.py
+++ b/solution.py
@@ -10,6 +10,8 @@
 D = 2048
 HEAD = 128
 LANES = 128
+SPLIT = 4
+LIMIT = 50 * 1024 * 1024
 MESH = pl.DeviceIdType.MESH
 
 
@@ -156,25 +158,31 @@
 def exchange_kernel(
     n_kv,
     first_writer,
-    tokens_ref,
-    gain_ref,
+    tokens_hbm,
+    gain_hbm,
     wq_hbm,
     wk_hbm,
     wv_hbm,
     wg_hbm,
     wo_hbm,
-    bias_ref,
+    bias_hbm,
     keys_hbm,
     values_hbm,
+    prefix_hbm,
+    accepted_hbm,
+    parent_hbm,
+    parts_ref,
+    fresh_ref,
+    keys,
+    values,
+    tokens_ref,
+    gain_ref,
+    parent_ref,
+    bias_ref,
     prefix_ref,
     accepted_ref,
-    parent_ref,
-    parts_ref,
-    fresh_ref,
     w_in,
     w_out,
-    keys,
-    values,
     partial,
     table,
     q_send,
@@ -211,21 +219,34 @@
         )
     pl.semaphore_signal(barrier, inc=1, device_id={"tp": 1 - core}, device_id_type=MESH)
 
-    loads = []
-    for place, (src, dst) in enumerate(
-        [
-            (wq_hbm, w_in.at[0]),
-            (wk_hbm, w_in.at[1]),
-            (wv_hbm, w_in.at[2]),
-            (wg_hbm, w_in.at[3]),
-            (keys_hbm, keys),
-            (values_hbm, values),
-            (wo_hbm, w_out),
-        ]
-    ):
+    def load(place, src, dst):
         copy = pltpu.make_async_copy(src, dst, local_sem.at[place])
         copy.start()
-        loads.append(copy)
+        return copy
+
+    small = [load(7, tokens_hbm, tokens_ref), load(8, gain_hbm, gain_ref)]
+    rows = columns // SPLIT
+    first = []
+    for piece in range(SPLIT):
+        span = pl.ds(piece * rows, rows)
+        first.append(load(13 + piece, wq_hbm.at[span], w_in.at[0, span]))
+    late = [
+        load(9, bias_hbm, bias_ref),
+        load(10, prefix_hbm, prefix_ref),
+        load(11, accepted_hbm, accepted_ref),
+        load(12, parent_hbm, parent_ref),
+    ]
+    loads = [None] + [
+        load(place, src, dst)
+        for place, src, dst in [
+            (1, wk_hbm, w_in.at[1]),
+            (2, wv_hbm, w_in.at[2]),
+            (3, wg_hbm, w_in.at[3]),
+            (4, keys_hbm, keys),
+            (5, values_hbm, values),
+            (6, wo_hbm, w_out),
+        ]
+    ]
 
     started = []
 
@@ -241,6 +262,8 @@
         copy.start()
         return copy
 
+    for copy in small:
+        copy.wait()
     flat = tokens_ref[...].astype(jnp.float32)
     square_part = jnp.sum(flat * flat, axis=1, keepdims=True)
     scaled = (flat * gain_ref[...]).astype(jnp.bfloat16)
@@ -249,7 +272,8 @@
         q_send[owner, :, group:] = square_lanes
 
     def project(which):
-        loads[which].wait()
+        for copy in first if which == 0 else [loads[which]]:
+            copy.wait()
         return jnp.dot(scaled, w_in[which], preferred_element_type=jnp.float32)
 
     part = project(0)
@@ -274,6 +298,8 @@
     cols = lax.broadcasted_iota(jnp.int32, (ctx, ctx), 1)
     table[...] = jnp.where(rows > cols, 1.0, 0.0).astype(jnp.bfloat16)
 
+    for copy in late:
+        copy.wait()
     place_p = lax.broadcasted_iota(jnp.int32, (props, props), 0)
     place_j = lax.broadcasted_iota(jnp.int32, (props, props), 1)
     reach = jnp.where(parent_ref[...] == place_p, 1.0, 0.0)
@@ -502,74 +528,92 @@
     parts_ref[1] = o_recv[...]
 
 
-CHUNKS = 4
+BLOCK = 64
 
 
 def cache_kernel(
     parts_ref,
     fresh_ref,
-    prefix_ref,
-    accepted_ref,
-    keys_hbm,
-    values_hbm,
+    keys,
+    values,
+    prefix_hbm,
+    accepted_hbm,
     mixed_ref,
     keys_out,
     values_out,
-    keys,
-    values,
-    in_sem,
+    patch,
+    prefix_ref,
+    accepted_ref,
+    scalar_sem,
     out_sem,
+    patch_sem,
 ):
     heads, ctx, head = keys.shape
     n_kv, props, wide = fresh_ref.shape
     own = heads // n_kv
-    step_heads = heads // CHUNKS
-    pairs = []
-    for chunk in range(CHUNKS):
-        span = pl.ds(chunk * step_heads, step_heads)
-        for side, (src, held, dst) in enumerate(
-            [(keys_hbm, keys, keys_out), (values_hbm, values, values_out)]
-        ):
-            copy = pltpu.make_async_copy(
-                src.at[span], held.at[span], in_sem.at[chunk, side]
-            )
-            copy.start()
-            back = pltpu.make_async_copy(
-                held.at[span], dst.at[span], out_sem.at[chunk, side]
-            )
-            pairs.append((chunk, side, held, copy, back))
+    window = 2 * BLOCK
+    blocks = ctx // BLOCK
+    scalars = [
+        pltpu.make_async_copy(prefix_hbm, prefix_ref, scalar_sem.at[0]),
+        pltpu.make_async_copy(accepted_hbm, accepted_ref, scalar_sem.at[1]),
+    ]
+    for copy in scalars:
+        copy.start()
     mixed_ref[...] = (
         parts_ref[0].astype(jnp.float32) + parts_ref[1].astype(jnp.float32)
     ).astype(jnp.bfloat16)
+    for copy in scalars:
+        copy.wait()
     start = prefix_ref[0] + accepted_ref[0] - lax.axis_index("kv") * ctx
-    window = 2 * props
-    base = pl.multiple_of(jnp.clip(start // props, 0, ctx // props - 2) * props, props)
-    touched = (start + props > 0) & (start < ctx)
+    first = jnp.clip(start // BLOCK, 0, blocks - 2)
+    base = pl.multiple_of(first * BLOCK, BLOCK)
+    sides = [(keys, keys_out), (values, values_out)]
+
+    def bulk(block, side):
+        held, dst = sides[side]
+        span = pl.ds(block * BLOCK, BLOCK)
+        return pltpu.make_async_copy(
+            held.at[:, span], dst.at[:, span], out_sem.at[block, side]
+        )
+
+    plain = [(block < first) | (block > first + 1) for block in range(blocks)]
+    for block in range(blocks):
+
+        @pl.when(plain[block])
+        def _(block=block):
+            for side in range(2):
+                bulk(block, side).start()
+
     row = lax.broadcasted_iota(jnp.int32, (window, props), 0) + base - start
     column = lax.broadcasted_iota(jnp.int32, (window, props), 1)
     picker = jnp.where(row == column, 1.0, 0.0).astype(jnp.bfloat16)
     offset = lax.broadcasted_iota(jnp.int32, (window, head), 0) + base - start
     inside = (offset >= 0) & (offset < props)
-    for chunk, side, held, copy, back in pairs:
+    patches = []
+    for side, (held, dst) in enumerate(sides):
+        for place in range(heads):
+            at = (side * own + place % own) * head
+            placed = jnp.dot(
+                picker,
+                fresh_ref[place // own, :, at : at + head],
+                preferred_element_type=jnp.float32,
+            )
+            now = held[place, pl.ds(base, window), :].astype(jnp.float32)
+            patch[side, place] = jnp.where(inside, placed, now).astype(jnp.bfloat16)
+        copy = pltpu.make_async_copy(
+            patch.at[side], dst.at[:, pl.ds(base, window)], patch_sem.at[side]
+        )
+        copy.start()
+        patches.append(copy)
+    for block in range(blocks):
+
+        @pl.when(plain[block])
+        def _(block=block):
+            for side in range(2):
+                bulk(block, side).wait()
+
+    for copy in patches:
         copy.wait()
-
-        @pl.when(touched)
-        def _(chunk=chunk, side=side, held=held):
-            for place in range(chunk * step_heads, (chunk + 1) * step_heads):
-                at = side * own * head + (place % own) * head
-                placed = jnp.dot(
-                    picker,
-                    fresh_ref[place // own, :, at : at + head],
-                    preferred_element_type=jnp.float32,
-                )
-                now = held[place, pl.ds(base, window), :].astype(jnp.float32)
-                held[place, pl.ds(base, window), :] = jnp.where(inside, placed, now).astype(
-                    jnp.bfloat16
-                )
-
-        back.start()
-    for chunk, side, held, copy, back in pairs:
-        back.wait()
 
 
 def fast(
@@ -599,23 +643,28 @@
     keys = jnp.transpose(cache_keys[0], (1, 0, 2))
     values = jnp.transpose(cache_values[0], (1, 0, 2))
     vmem = pl.BlockSpec(memory_space=pltpu.VMEM)
-    smem = pl.BlockSpec(memory_space=pltpu.SMEM)
     hbm = pl.BlockSpec(memory_space=pl.ANY)
     low = jnp.bfloat16
     cache_shape = (heads, ctx, HEAD)
-    parts, fresh = pl.pallas_call(
+    parts, fresh, keys_held, values_held = pl.pallas_call(
         functools.partial(exchange_kernel, n_kv, first_writer),
         out_shape=(
             jax.ShapeDtypeStruct((2, props, out_columns), low),
             jax.ShapeDtypeStruct((n_kv, props, 2 * group), low),
+            jax.ShapeDtypeStruct(cache_shape, low),
+            jax.ShapeDtypeStruct(cache_shape, low),
         ),
-        in_specs=[vmem, vmem, hbm, hbm, hbm, hbm, hbm, smem, hbm, hbm, smem, smem, vmem],
-        out_specs=(vmem, vmem),
+        in_specs=[hbm] * 13,
+        out_specs=(vmem,) * 4,
         scratch_shapes=[
+            pltpu.VMEM((props, columns), low),
+            pltpu.VMEM((1, columns), jnp.float32),
+            pltpu.VMEM((1, props), jnp.int32),
+            pltpu.SMEM((heads,), jnp.float32),
+            pltpu.SMEM((1,), jnp.int32),
+            pltpu.SMEM((1,), jnp.int32),
             pltpu.VMEM((4, columns, width), low),
             pltpu.VMEM((width, out_columns), low),
-            pltpu.VMEM(cache_shape, low),
-            pltpu.VMEM(cache_shape, low),
             pltpu.VMEM((n_kv, props, 4 * group), jnp.float32),
             pltpu.VMEM((ctx, ctx), low),
             pltpu.VMEM((n_kv, props, group + LANES), low),
@@ -632,12 +681,12 @@
             pltpu.VMEM((n_kv, props, 2 * group), low),
             pltpu.VMEM((props, out_columns), low),
             pltpu.VMEM((props, out_columns), low),
-            pltpu.SemaphoreType.DMA((7,)),
+            pltpu.SemaphoreType.DMA((13 + SPLIT,)),
             pltpu.SemaphoreType.DMA((7, n_kv)),
             pltpu.SemaphoreType.DMA((7, n_kv)),
         ],
         compiler_params=pltpu.CompilerParams(
-            collective_id=0, has_side_effects=True, vmem_limit_bytes=40 * 1024 * 1024
+            collective_id=0, has_side_effects=True, vmem_limit_bytes=LIMIT
         ),
         name="exchange",
     )(
@@ -662,17 +711,19 @@
             jax.ShapeDtypeStruct(cache_shape, low),
             jax.ShapeDtypeStruct(cache_shape, low),
         ),
-        in_specs=[vmem, vmem, smem, smem, hbm, hbm],
+        in_specs=[vmem] * 4 + [hbm] * 2,
         out_specs=(vmem, hbm, hbm),
         scratch_shapes=[
-            pltpu.VMEM(cache_shape, low),
-            pltpu.VMEM(cache_shape, low),
-            pltpu.SemaphoreType.DMA((CHUNKS, 2)),
-            pltpu.SemaphoreType.DMA((CHUNKS, 2)),
+            pltpu.VMEM((2, heads, 2 * BLOCK, HEAD), low),
+            pltpu.SMEM((1,), jnp.int32),
+            pltpu.SMEM((1,), jnp.int32),
+            pltpu.SemaphoreType.DMA((2,)),
+            pltpu.SemaphoreType.DMA((ctx // BLOCK, 2)),
+            pltpu.SemaphoreType.DMA((2,)),
         ],
         compiler_params=pltpu.CompilerParams(vmem_limit_bytes=16 * 1024 * 1024),
         name="cache",
-    )(parts, fresh, prefix_len, accepted, keys, values)
+    )(parts, fresh, keys_held, values_held, prefix_len, accepted)
     return (
         mixed[None],
         jnp.transpose(keys_next, (1, 0, 2))[None],
@@ -685,7 +736,7 @@
 
     def body(*arrays):
         seqs, heads, ctx = arrays[0].shape[0], arrays[8].shape[2], arrays[8].shape[1]
-        fits = heads % n_kv == 0 and heads % CHUNKS == 0 and seqs == 1 and n_tp == 2
+        fits = heads % n_kv == 0 and seqs == 1 and n_tp == 2
         if fits and n_kv % 4 == 0 and ctx % 128 == 0:
             return fast(n_kv, *arrays)
         return local(*arrays)

time: 42.9 us -> 31.4 us (0.73)
  local copies, waits for them, and re-layouts: 12.6 us -> 2.7 us
  Pallas kernels: 27.9 us -> 26.5 us
    unnamed x22 -> x8, local copies, waits for them, and re-layouts: 12.6 us -> 2.7 us
    pallas_call x1, Pallas kernels: 3.92 us -> 3 us  [fast(): pl.pallas_call(cache_kernel, out_shape=(jax.ShapeDtypeStruct((props, out_...]
    pallas_call x1, Pallas kernels: 24 us -> 23.5 us  [fast(): pl.pallas_call(functools.partial(exchange_kernel, n_kv, first_writer), ou...]
where the time goes in v2:
time: 31.4 us; the launch traced here: 31.1 us
  Pallas kernels  26.5 us (84%)
  local copies, waits for them, and re-layouts  2.7 us (9%)
  between operations  1.95 us (6%)
    pallas_call x1, Pallas kernels, fast(): pl.pallas_call(functools.partial(exchange_kernel, n_kv, first_writer), ou...  23.5 us
    pallas_call x1, Pallas kernels, fast(): pl.pallas_call(cache_kernel, out_shape=(jax.ShapeDtypeStruct((props, out_...  3 us
    unnamed x8, local copies, waits for them, and re-layouts  2.7 us

profile of v2, /device:TPU:0, one launch (start us, length us, event | category | flops | bytes accessed | tf_op | source)
XLA Modules:
  0.0 31.1 jit_solution(13920960570107675349)
XLA Ops:
  1.9 0.0 copy-start
  1.9 0.7 %copy-done = bf16[1,16,512]{2,1,0:T(8,128)(2,1)S(1)} copy-done((bf16[1,16,512]{2,1,0:T(8,128)(2,1)S(1)}, bf16[1,16,512]{2,1,0:T(8,128)(2,1)}, u32[]{:S(2)}) %copy-start) | copy-done | bytes 16408
  2.6 0.0 copy-start.1
  2.6 0.7 %copy-done.1 = f32[512]{0:T(512)S(1)} copy-done((f32[512]{0:T(512)S(1)}, f32[512]{0:T(512)}, u32[]{:S(2)}) %copy-start.1) | copy-done | bytes 2072
  3.3 0.0 copy-start.2
  3.3 0.7 %copy-done.2 = f32[12]{0:T(128)S(1)} copy-done((f32[12]{0:T(128)S(1)}, f32[12]{0:T(128)}, u32[]{:S(2)}) %copy-start.2) | copy-done | bytes 72
  4.0 0.0 copy-start.3
  4.0 0.7 %copy-done.3 = s32[1,16]{1,0:T(1,128)S(1)} copy-done((s32[1,16]{1,0:T(1,128)S(1)}, s32[1,16]{1,0:T(1,128)}, u32[]{:S(2)}) %copy-start.3) | copy-done | bytes 88
  4.6 23.5 %exchange.1 = (bf16[2,16,512]{2,1,0:T(8,128)(2,1)S(1)}, bf16[4,16,768]{2,1,0:T(8,128)(2,1)S(1)}, bf16[12,512,128]{2,1,0:T(8,128)(2,1)S(1)}, bf16[12,512,128]{2,1,0:T(8,128)(2,1)S(1)}) custom-call(bf16[16,512]{1,0:T(8,128)(2,1)S(1)} %bitcast.15, f32[1,512]{1,0:T(1,128)S(1)} %bitcast.16, bf16[512,1536]{1,0:T(8,128)(2,1)} %wq_hbm.1, bf16[512,1536]{1,0:T(8,128)(2,1)} %wk_hbm.1, ...), custom_call_target="tpu_custom_call" | custom-call | tf_op jit(solution)/shard_map/exchange/pallas_call | solution.py:649
  28.1 3.0 %cache.1 = (bf16[16,512]{1,0:T(8,128)(2,1)}, bf16[12,512,128]{2,1,0:T(8,128)(2,1)}, bf16[12,512,128]{2,1,0:T(8,128)(2,1)}) custom-call(bf16[2,16,512]{2,1,0:T(8,128)(2,1)S(1)} %get-tuple-element.10.parts_ref, bf16[4,16,768]{2,1,0:T(8,128)(2,1)S(1)} %get-tuple-element.11.fresh_ref, bf16[12,512,128]{2,1,0:T(8,128)(2,1)S(1)} %get-tuple-element.12.keys, ...), custom_call_target="tpu_custom_call" | custom-call | tf_op jit(solution)/shard_map/cache/pallas_call | solution.py:707
Async XLA Ops:
  1.9 0.7 %copy-start = (bf16[1,16,512]{2,1,0:T(8,128)(2,1)S(1)}, bf16[1,16,512]{2,1,0:T(8,128)(2,1)}, u32[]{:S(2)}) copy-start(bf16[1,16,512]{2,1,0:T(8,128)(2,1)} %param.13) | copy-start | bytes 49156
  2.6 0.7 %copy-start.1 = (f32[512]{0:T(512)S(1)}, f32[512]{0:T(512)}, u32[]{:S(2)}) copy-start(f32[512]{0:T(512)} %param.14) | copy-start | bytes 6148
  3.3 0.7 %copy-start.2 = (f32[12]{0:T(128)S(1)}, f32[12]{0:T(128)}, u32[]{:S(2)}) copy-start(f32[12]{0:T(128)} %bias_hbm.1) | copy-start | bytes 148
  4.0 0.7 %copy-start.3 = (s32[1,16]{1,0:T(1,128)S(1)}, s32[1,16]{1,0:T(1,128)}, u32[]{:S(2)}) copy-start(s32[1,16]{1,0:T(1,128)} %parent_hbm.1) | copy-start | bytes 196
